TPU v7x, 512 devices: a whole 4x4x16 slice. The times are simulated.
512 devices in a mesh: sp: 16 (over z), fs: 4 (over y), tp: 8 (over x, core).
Axes of the slice: x: 4, y: 4, z: 16, core: 2. Of those that a mesh axis runs over, the one named last changes fastest.
Arguments:
- tokens: bfloat16 [4, 8192, 2048], P('fs', 'sp', 'tp'), may hold values from -6 to 6
- norm_gain: float32 [2048], replicated, may hold values from 0.1 to 1.9
- query_weight: bfloat16 [2048, 1024], P(('sp', 'fs'), 'tp'), may hold values from -0.125 to 0.125
- key_weight: bfloat16 [2048, 1024], P(('sp', 'fs'), 'tp'), may hold values from -0.125 to 0.125
- value_weight: bfloat16 [2048, 2048], P(('sp', 'fs'), 'tp'), may hold values from -0.125 to 0.125
- outgate_weight: bfloat16 [2048, 2048], P(('sp', 'fs'), 'tp'), may hold values from -0.125 to 0.125
- gate_weight: bfloat16 [2048, 2, 16], P(('sp', 'fs'), None, 'tp'), may hold values from -6 to 6
- forget_bias: float32 [16], P('tp')
- forget_shift: float32 [4, 16, 8192], P('fs', 'tp', 'sp'), may hold values from -1.5 to 0
- head_norm_gain: float32 [2048], P('tp'), may hold values from 0.1 to 1.9
- exit_weight: bfloat16 [2048, 2048], P(('sp', 'fs'), 'tp'), may hold values from -0.125 to 0.125
- entry_weight: bfloat16 [2048, 2048], P(('sp', 'fs'), 'tp'), may hold values from -0.125 to 0.125
- signal_weight: bfloat16 [2048, 2048], P(('sp', 'fs'), 'tp'), may hold values from -0.125 to 0.125
- conv_kernel: float32 [3, 2048], P(None, 'tp'), may hold values from -3.5 to 3.5
- merge_weight: bfloat16 [4096, 2048], P(('sp', 'fs'), 'tp'), may hold values from -0.09375 to 0.09375
Outputs:
- mixed: bfloat16 [4, 8192, 2048], P('fs', 'sp', 'tp')
All inputs are finite; a program needn't handle non-finite values.
Results may differ from a plain program's by a relative error of at most 0.017.
The roundings to bfloat16 on the way count: a program that leaves them out, or rounds other values in their place, can miss the bound.
Values may be sent and summed in bfloat16 or wider, within the bound.
A program may use at most 64 MiB of HBM per device.

v0:
```python
import jax
import jax.numpy as jnp
from jax import lax
from jax.sharding import Mesh
from jax.sharding import PartitionSpec as P

DK = 64
DV = 128
BLOCK = 128
KERNEL = 3
TP = ("tp_0", "tp_1")


EPSILON = 1e-06
EMPTY_LOG = -1e30
HIGHEST = lax.Precision.HIGHEST


def from_everyone(array, axis):
    copies = jnp.broadcast_to(array, (lax.axis_size(axis), *array.shape))
    return lax.all_to_all(copies, axis, split_axis=0, concat_axis=0, tiled=True)


def gathered_once(array, axis):
    leaves = jax.tree.leaves(array)
    order = sorted(range(len(leaves)), key=lambda k: -leaves[k].size)
    width = (1, *leaves[order[0]].shape)[-1]
    lines = [
        jnp.pad(leaves[k].reshape(-1), (0, -leaves[k].size % width)).reshape(-1, width)
        for k in order
    ]
    both, at, found = (from_everyone(jnp.concatenate(lines), axis), 0, {})
    for k, line in zip(order, lines):
        piece = both[:, at : at + len(line)].reshape(len(both), -1)
        found[k] = piece[:, : leaves[k].size].reshape(-1, *leaves[k].shape)
        at += len(line)
    numbers = iter(range(len(leaves)))
    return jax.tree.map(lambda _: found[next(numbers)], array)


def joined_by_halves(pieces, combine):
    while len(jax.tree.leaves(pieces)[0]) > 1:
        pieces = jax.vmap(combine)(
            *(jax.tree.map(lambda part: part[side::2], pieces) for side in (0, 1))
        )
    return jax.tree.map(lambda part: part[0], pieces)


def carried_in(array, axis, combine, identity):
    peers, position = (lax.axis_size(axis), lax.axis_index(axis))
    passed = jnp.arange(peers) < position

    def kept(part, zero, own):
        part = jnp.where(
            passed.reshape(-1, *(1 for _ in own.shape)), part, jnp.asarray(zero, own.dtype)
        )
        return part

    pieces = gathered_once(array, axis)
    return joined_by_halves(jax.tree.map(kept, pieces, identity, array), combine)


def in_order(parts, dim):
    dims = list(parts.shape[1:])
    dims[dim] *= parts.shape[0]
    return jnp.moveaxis(parts, 0, dim).reshape(dims)


def gathered_by_axis(array, axes, dim):
    far, near = axes
    parts = from_everyone(from_everyone(array, far), near)
    return in_order(parts.swapaxes(0, 1).reshape(-1, *array.shape), dim)


def passed_along(value, axis, steps):
    count = lax.axis_size(axis)
    initial, last = (max(0, -steps), min(count, count - steps))
    return lax.ppermute(value, axis, [(source, source + steps) for source in range(initial, last)])


def sent_together(arrays, axis, dim, along):
    both = jnp.concatenate(arrays, axis=along)
    filled, at, done = (gathered_by_axis(both, axis, dim), 0, [])
    for a in arrays:
        done.append(lax.slice_in_dim(filled, at, at + a.shape[along], axis=along))
        at += a.shape[along]
    return tuple(done)


def whole_of(array, axes, dim):
    for axis in reversed(axes):
        array = lax.all_gather(array, axis, axis=dim, tiled=True)
    return array


def combine(earlier, later):
    ceiling = jnp.maximum(later[2] + earlier[1], later[1])
    kept = jnp.exp(later[2] + earlier[1] - ceiling)
    added = jnp.exp(later[1] - ceiling)
    state = kept[..., None, None] * earlier[0] + added[..., None, None] * later[0]
    return (state, ceiling, earlier[2] + later[2])


def identity_state(heads):
    return (
        jnp.zeros((heads, DK, DV), jnp.float32),
        jnp.full((heads,), EMPTY_LOG, jnp.float32),
        jnp.zeros((heads,), jnp.float32),
    )


def add_product(left, piece):
    return jnp.dot(left, piece, preferred_element_type=jnp.float32)


def split_columns(total, stack):
    outputs = []
    offset = 0
    for weight in stack:
        outputs.append(total[:, offset : offset + weight.shape[1]])
        offset = offset + weight.shape[1]
    return outputs


def incoming_state(running):
    heads = running[1].shape[0]
    before = carried_in((running[0], running[1], running[2]), "sp", combine, identity_state(heads))
    ceiling = jnp.maximum(before[1], before[2])
    shrink = jnp.exp(before[1] - ceiling)
    return (before[0] * shrink[:, None, None], ceiling, before[2])


def memory_states(keys, values, gates, forget_bias, forget_shift):
    count = gates.shape[0]
    heads = forget_bias.shape[0]
    blocks = count // BLOCK
    inputs = gates[:, :heads].reshape(blocks, BLOCK, heads)
    logs = jax.nn.log_sigmoid(gates[:, heads:] + forget_bias) + forget_shift[0].T
    cumulative = jnp.cumsum(logs.reshape(blocks, BLOCK, heads), axis=1)
    last = cumulative[:, -1]
    weight_logs = last[:, None, :] - cumulative + inputs
    peak = jnp.max(weight_logs, axis=1)
    coefficient_array = jnp.exp(weight_logs - peak[:, None, :])
    scaled = keys.reshape(blocks, BLOCK, heads, DK).astype(jnp.float32) * DK ** (-0.5)
    value_float = values.reshape(blocks, BLOCK, heads, DV).astype(jnp.float32)
    states = jnp.einsum(
        "csh,cshk,cshv->chkv", coefficient_array, scaled, value_float, precision=HIGHEST
    )
    running = identity_state(heads)
    prefixes = []
    for index in range(blocks):
        prefixes.append(running)
        running = combine(running, (states[index], peak[index], last[index]))
    leading_part = tuple((jnp.stack([item[member] for item in prefixes]) for member in range(3)))
    gate_apertures = combine(incoming_state(running), leading_part)
    return (gate_apertures, cumulative, inputs)


def memory_output(
    queries, keys, values, outgates, inputs, cumulative, gate_apertures, head_norm_gain
):
    blocks = cumulative.shape[0]
    heads = cumulative.shape[2]
    count = queries.shape[0]
    query_blocks = queries.reshape(blocks, BLOCK, heads, DK)
    key_blocks = keys.reshape(blocks, BLOCK, heads, DK)
    value_blocks = values.reshape(blocks, BLOCK, heads, DV)
    score_matrix = jnp.einsum(
        "cjhk,cshk->chjs", query_blocks, key_blocks, preferred_element_type=jnp.float32
    ) * DK ** (-0.5)
    cum_lanes = cumulative.transpose(0, 2, 1)
    input_lanes = inputs.transpose(0, 2, 1)
    causal = jnp.tril(jnp.ones((BLOCK, BLOCK), dtype=bool))
    decay = jnp.where(
        causal,
        cum_lanes[..., :, None] - cum_lanes[..., None, :] + input_lanes[..., None, :],
        -jnp.inf,
    )
    inter = cum_lanes + gate_apertures[1][..., None]
    ceiling = jnp.maximum(inter, jnp.max(decay, axis=-1))
    weighted = score_matrix * jnp.exp(decay - ceiling[..., None])
    numerator = jnp.einsum(
        "chjs,cshv->chjv",
        weighted.astype(jnp.bfloat16),
        value_blocks,
        preferred_element_type=jnp.float32,
    )
    query_float = query_blocks.astype(jnp.float32)
    carried = jnp.exp(inter - ceiling)
    numerator = numerator + carried[..., None] * jnp.einsum(
        "cjhk,chkv->chjv", query_float, gate_apertures[0], precision=HIGHEST
    )
    result = numerator * lax.rsqrt(
        jnp.mean(numerator * numerator, axis=-1, keepdims=True) + EPSILON
    )
    result = result.transpose(0, 2, 1, 3).reshape(count, heads * DV) * head_norm_gain
    return (result * jax.nn.sigmoid(outgates.astype(jnp.float32))).astype(jnp.bfloat16)


def local(
    tokens,
    norm_gain,
    query_weight,
    key_weight,
    value_weight,
    outgate_weight,
    gate_weight,
    forget_bias,
    forget_shift,
    head_norm_gain,
    exit_weight,
    entry_weight,
    signal_weight,
    conv_kernel,
    merge_weight,
):
    whole = gathered_by_axis(tokens, ("tp_0", "tp_1"), 2)[0]
    count = whole.shape[0]
    flat = whole.astype(jnp.float32)
    normed = (
        flat * lax.rsqrt(jnp.mean(flat * flat, axis=-1, keepdims=True) + EPSILON) * norm_gain
    ).astype(jnp.bfloat16)
    gate_rows = gate_weight.reshape(gate_weight.shape[0], -1)
    state_stack = [key_weight, value_weight, gate_rows]
    other_stack = [query_weight, outgate_weight, exit_weight, entry_weight, signal_weight]
    stacked = jnp.concatenate(state_stack + other_stack, axis=1)
    total = add_product(normed, lax.all_gather(stacked, ("sp", "fs"), axis=0, tiled=True))
    columns = split_columns(total, state_stack + other_stack)
    keys = columns[0].astype(jnp.bfloat16)
    values = columns[1].astype(jnp.bfloat16)
    gate_apertures, cumulative, inputs = memory_states(
        keys, values, columns[2], forget_bias, forget_shift
    )
    others = columns[3:]
    queries = others[0].astype(jnp.bfloat16)
    outgates = others[1].astype(jnp.bfloat16)
    exit_rows = others[2].astype(jnp.bfloat16)
    entry_rows = others[3].astype(jnp.bfloat16)
    signal_rows = others[4].astype(jnp.bfloat16)
    mixed_in = (entry_rows.astype(jnp.float32) * signal_rows.astype(jnp.float32)).astype(
        jnp.bfloat16
    )
    rim = passed_along(mixed_in[count - (KERNEL - 1) :], "sp", 1)
    padded = jnp.concatenate([rim, mixed_in], axis=0).astype(jnp.float32)
    response = conv_kernel[0] * padded[0:count]
    for tap in range(1, KERNEL):
        response = response + conv_kernel[tap] * padded[tap : tap + count]
    conv_out = (exit_rows.astype(jnp.float32) * response).astype(jnp.bfloat16)
    memory_out = memory_output(
        queries, keys, values, outgates, inputs, cumulative, gate_apertures, head_norm_gain
    )
    memory_all, conv_all = sent_together((memory_out, conv_out), ("tp_0", "tp_1"), 1, 0)
    concatenated_result = jnp.concatenate([memory_all, conv_all], axis=1)
    mixed = add_product(concatenated_result, whole_of(merge_weight, ("sp", "fs"), 0))
    return mixed.astype(jnp.bfloat16)[None]


def solution(mesh):
    torus = Mesh(
        mesh.devices.reshape(mesh.shape["sp"], mesh.shape["fs"], 4, 2), ("sp", "fs", "tp_0", "tp_1")
    )
    in_specs = (
        P("fs", "sp", TP),
        P(),
        P(("sp", "fs"), TP),
        P(("sp", "fs"), TP),
        P(("sp", "fs"), TP),
        P(("sp", "fs"), TP),
        P(("sp", "fs"), None, TP),
        P(TP),
        P("fs", TP, "sp"),
        P(TP),
        P(("sp", "fs"), TP),
        P(("sp", "fs"), TP),
        P(("sp", "fs"), TP),
        P(None, TP),
        P(("sp", "fs"), TP),
    )
    out_specs = P("fs", "sp", TP)
    return jax.shard_map(local, mesh=torus, in_specs=in_specs, out_specs=out_specs, check_vma=False)
```

profile of v0, /device:TPU:1, one launch (start us, length us, event | category | flops | bytes accessed | tf_op | source)
XLA Modules:
  0.0 306.6 jit_solution(729016437624423963)
XLA Ops:
  7.4 0.8 copy.87
  8.1 1.6 concatenate.40
  9.7 1.0 broadcast_in_dim.50
  10.8 15.2 %all_to_all.28 = bf16[4,1,512,256]{3,2,1,0:T(8,128)(2,1)S(1)} all-to-all(bf16[4,1,512,256]{3,2,1,0:T(8,128)(2,1)S(1)} %broadcast_in_dim.50), channel_id=1, replica_groups=mesh['sp'=16,'fs'=4,'tp_0'=4,'tp_1'=2] {'tp_0'}, dimensions={0} | all-to-all | bytes 2097152 | tf_op jit(solution)/shard_map/all_to_all | solution.py:21
  26.1 10.5 %all_to_all.29 = bf16[2,4,1,512,256]{4,3,1,2,0:T(8,128)(2,1)S(1)} all-to-all(bf16[2,4,1,512,256]{4,3,1,2,0:T(8,128)(2,1)S(1)} %broadcast_in_dim.51), channel_id=1, replica_groups=mesh['sp'=16,'fs'=4,'tp_0'=4,'tp_1'=2] {'tp_1'}, dimensions={0} | all-to-all | bytes 4194304 | tf_op jit(solution)/shard_map/all_to_all | solution.py:21
  36.6 2.4 copy_convert_fusion
  39.1 5.4 %copy.86 = f32[1,512,8,256]{1,3,2,0:T(8,128)} copy(f32[1,512,8,256]{3,1,2,0:T(8,128)} %bitcast.208) | data formatting | bytes 8388608 | tf_op jit(solution)/shard_map/convert_element_type | solution.py:219
  44.4 0.5 multiply_reduce_fusion
  45.1 2.6 fusion.5
  47.8 112.6 %all-gather.3.cloned.1.call-done = bf16[2048,1540]{1,0:T(8,128)(2,1)} async-done(((bf16[32,1540]{1,0:T(8,128)(2,1)}), bf16[2048,1540]{1,0:T(8,128)(2,1)}) %all-gather.3.cloned.1.call-update) | async-done | bytes 6307856 | tf_op jit(solution)/shard_map/all_gather | solution.py:227
  160.4 7.8 %fusion.98 = (bf16[512,1540]{0,1:T(8,128)(2,1)}, f32[512,1540]{0,1:T(8,128)S(1)}) fusion(bf16[512,2048]{0,1:T(8,128)(2,1)S(1)} %fusion.5, bf16[2048,1540]{1,0:T(8,128)(2,1)} %all-gather.3.cloned.1.call-done), kind=kOutput, calls=%fused_computation.173 | convolution fusion | flops 3230402560 | bytes 13135872 | tf_op jit(solution)/shard_map/dot_general | solution.py:113
  169.1 0.6 copy-done
  170.7 0.6 fusion.37
  171.4 0.7 multiply_add_fusion.3
  172.8 1.1 broadcast_in_dim.57
  173.8 6.9 %all-to-all-start.2 = ((f32[16,130,128]{2,1,0:T(8,128)}), f32[16,130,128]{2,1,0:T(8,128)S(1)}, u32[]{:S(2)}, u32[]{:S(2)}) async-start(f32[16,130,128]{2,1,0:T(8,128)} %broadcast_in_dim.57), calls=%async_computation.2 | async-start | bytes 2228224 | tf_op jit(solution)/shard_map/all_to_all | solution.py:21
  180.9 9.8 %all_gather.10 = bf16[256,256]{1,0:T(8,128)(2,1)} all-gather(bf16[64,256]{1,0:T(8,128)(2,1)S(1)} %copy-done.12), channel_id=1, replica_groups=mesh['sp'=16,'fs'=4,'tp_0'=4,'tp_1'=2] {'fs'}, dimensions={0}, use_global_device_ids=true | all-gather | bytes 163840 | tf_op jit(solution)/shard_map/all_gather | solution.py:92
  191.0 0.4 fusion.25
  191.5 0.7 reshape.564
  192.2 33.2 %all-to-all-done.2 = f32[16,130,128]{2,1,0:T(8,128)S(1)} async-done(((f32[16,130,128]{2,1,0:T(8,128)}), f32[16,130,128]{2,1,0:T(8,128)S(1)}, u32[]{:S(2)}, u32[]{:S(2)}) %all-to-all-start.2) | async-done | bytes 1064992 | tf_op jit(solution)/shard_map/all_to_all | solution.py:21
  225.6 0.6 subtract_exponential_fusion.2
  226.3 0.6 subtract_exponential_fusion.5
  226.9 0.6 subtract_exponential_fusion.8
  227.5 0.6 exponential_bitcast_fusion.1
  228.1 0.5 exponential_bitcast_fusion
  228.7 0.5 fusion.74
  229.2 0.5 subtract_exponential_fusion.7
  229.7 0.6 subtract_exponential_fusion.4
  230.3 0.6 subtract_exponential_fusion.1
  230.9 0.7 subtract_exponential_fusion.6
  231.6 0.7 copy.102
  232.2 0.6 subtract_exponential_fusion.3
  232.9 0.7 copy.107
  233.6 0.8 subtract_exponential_fusion
  234.4 0.6 copy.104
  235.0 0.6 copy.109
  236.8 0.7 fusion.28
  237.5 1.4 multiply_reduce_fusion.1
  239.0 0.3 copy.110
  239.7 3.2 %collective-permute-start = (bf16[2,256]{0,1:T(8,128)(2,1)S(1)}, bf16[2,256]{0,1:T(8,128)(2,1)S(1)}, u32[]{:S(2)}, u32[]{:S(2)}) collective-permute-start(bf16[2,256]{0,1:T(8,128)(2,1)S(1)} %slice.297), channel_id=1, source_target_pairs={{0,32},{32,64},{64,96},{96,128},{128,160},{160,192},{192,224},{224... | collective-permute-start | bytes 3080 | tf_op jit(solution)/shard_map/ppermute | solution.py:78
  243.0 1.6 collective-permute-done
  244.7 0.5 fusion.19
  245.6 21.7 %all_to_all.30 = bf16[4,1024,256]{2,1,0:T(8,128)(2,1)S(1)} all-to-all(bf16[4,1024,256]{2,1,0:T(8,128)(2,1)S(1)} %broadcast_in_dim.62), channel_id=1, replica_groups=mesh['sp'=16,'fs'=4,'tp_0'=4,'tp_1'=2] {'tp_0'}, dimensions={0} | all-to-all | bytes 4194304 | tf_op jit(solution)/shard_map/all_to_all | solution.py:21
  267.6 18.4 %all_to_all.31 = bf16[2,4,1024,256]{3,2,1,0:T(8,128)(2,1)S(1)} all-to-all(bf16[2,4,1024,256]{3,2,1,0:T(8,128)(2,1)S(1)} %broadcast_in_dim.104), channel_id=1, replica_groups=mesh['sp'=16,'fs'=4,'tp_0'=4,'tp_1'=2] {'tp_1'}, dimensions={0} | all-to-all | bytes 8388608 | tf_op jit(solution)/shard_map/all_to_all | solution.py:21
  286.3 1.7 fusion.90
  288.0 3.9 %copy.113 = bf16[512,8,256]{0,2,1:T(8,128)(2,1)} copy(bf16[512,8,256]{2,0,1:T(8,128)(2,1)} %get-tuple-element.28) | data formatting | bytes 4194304 | tf_op jit(solution)/shard_map/slice | solution.py:85
  291.9 2.4 copy.114
  294.3 4.9 %fusion.11 = bf16[1,512,256]{2,1,0:T(8,128)(2,1)} fusion(bf16[4096,256]{1,0:T(8,128)(2,1)} %all-gather.5.cloned.1.call-done, bf16[512,2048]{0,1:T(8,128)(2,1)} %bitcast.213, bf16[512,2048]{0,1:T(8,128)(2,1)} %bitcast.212), kind=kOutput, calls=%fused_computation.13 | convolution fusion | flops 1082261504 | bytes 6553600 | tf_op jit(solution)/shard_map/dot_general | solution.py:113
  (156 shorter events, 6.3 us)
Async XLA Ops:
  7.4 153.0 %all-gather.3.cloned.1.call-start = ((), (), s32[]{:S(2)}) async-start(), calls=%async_computation.5 | async-start | bytes 6922240 | tf_op jit(solution)/shard_map/all_gather | solution.py:227
  44.4 0.7 copy-start.17
  47.7 120.5 %copy-start.24 = (f32[1,2,512]{2,1,0:T(2,128)S(1)}, f32[1,2,512]{2,1,0:T(2,128)}, u32[]{:S(2)}) copy-start(f32[1,2,512]{2,1,0:T(2,128)} %param.23) | copy-start | bytes 12292
  47.8 120.5 %copy-start.34 = (f32[2]{0:T(128)S(1)}, f32[2]{0:T(128)}, u32[]{:S(2)}) copy-start(f32[2]{0:T(128)} %param.22) | copy-start | bytes 28
  168.2 1.4 copy-start
  169.9 4.0 %copy-start.3 = (bf16[4,128,2,64]{1,0,3,2:T(4,128)(2,1)}, bf16[4,128,2,64]{1,0,3,2:T(4,128)(2,1)S(1)}, u32[]{:S(2)}) copy-start(bf16[4,128,2,64]{1,0,3,2:T(4,128)(2,1)S(1)} %reshape.565) | copy-start | bytes 393220
  169.9 3.9 %copy-start.1 = (bf16[4,128,2,128]{1,0,3,2:T(4,128)(2,1)}, bf16[4,128,2,128]{1,0,3,2:T(4,128)(2,1)S(1)}, u32[]{:S(2)}) copy-start(bf16[4,128,2,128]{1,0,3,2:T(4,128)(2,1)S(1)} %reshape.568) | copy-start | bytes 786436
  172.1 8.8 %copy-start.12 = (bf16[64,256]{1,0:T(8,128)(2,1)S(1)}, bf16[64,256]{1,0:T(8,128)(2,1)}, u32[]{:S(2)}) copy-start(bf16[64,256]{1,0:T(8,128)(2,1)} %param.29) | copy-start | bytes 98308
  173.8 51.5 %all-to-all-start.2 = ((f32[16,130,128]{2,1,0:T(8,128)}), f32[16,130,128]{2,1,0:T(8,128)S(1)}, u32[]{:S(2)}, u32[]{:S(2)}) async-start(f32[16,130,128]{2,1,0:T(8,128)} %broadcast_in_dim.57), calls=%async_computation.2 | async-start | bytes 2228224 | tf_op jit(solution)/shard_map/all_to_all | solution.py:21
  180.8 113.5 %all-gather.5.cloned.1.call-start = ((), (), s32[]{:S(2)}) async-start(), calls=%async_computation.6 | async-start | bytes 2228224 | tf_op jit(solution)/shard_map/all_gather | solution.py:92
  190.8 41.5 %copy-start.28 = (f32[4]{0:T(128)}, f32[4]{0:T(128)S(1)}, u32[]{:S(2)}) copy-start(f32[4]{0:T(128)S(1)} %pad.26.clone) | copy-start | bytes 52
  190.8 41.4 %copy-start.26 = (pred[16]{0:T(512)(128)(4,1)}, pred[16]{0:T(512)(128)(4,1)S(1)}, u32[]{:S(2)}) copy-start(pred[16]{0:T(512)(128)(4,1)S(1)} %iota_compare_fusion.1) | copy-start | bytes 52
  190.8 41.4 %copy-start.8 = (pred[128,128]{1,0:T(8,128)(4,1)}, pred[128,128]{1,0:T(8,128)(4,1)S(1)}, u32[]{:S(2)}) copy-start(pred[128,128]{1,0:T(8,128)(4,1)S(1)} %iota_compare_fusion) | copy-start | bytes 49156
  190.9 34.7 %copy-start.10 = (f32[4,2,128]{2,1,0:T(2,128)}, f32[4,2,128]{2,1,0:T(2,128)S(1)}, u32[]{:S(2)}) copy-start(f32[4,2,128]{2,1,0:T(2,128)S(1)} %copy.92) | copy-start | bytes 12292
  190.9 34.5 %copy-start.16 = (f32[4,2,128]{2,1,0:T(2,128)}, f32[4,2,128]{2,1,0:T(2,128)S(1)}, u32[]{:S(2)}) copy-start(f32[4,2,128]{2,1,0:T(2,128)S(1)} %copy.94) | copy-start | bytes 12292
  191.4 40.9 %copy-start.9 = (f32[4,2,128]{2,1,0:T(2,128)}, f32[4,2,128]{2,1,0:T(2,128)S(1)}, u32[]{:S(2)}) copy-start(f32[4,2,128]{2,1,0:T(2,128)S(1)} %fusion.25) | copy-start | bytes 12292
  232.9 2.8 copy-start.27
  235.5 0.7 copy-start.14
  235.6 0.7 copy-start.15
  235.7 0.7 copy-start.20
  235.7 0.7 copy-start.21
  235.7 0.8 copy-start.22
  235.7 0.8 copy-start.23
  235.7 0.9 copy-start.30
  235.7 0.9 copy-start.31
  235.7 0.9 copy-start.32
  235.7 1.0 copy-start.5
  235.7 1.0 copy-start.6
  235.8 1.0 copy-start.7
  235.8 1.0 copy-start.18
  235.8 1.0 copy-start.19
  235.8 1.0 copy-start.29
  235.9 1.5 copy-start.2
  235.9 1.5 copy-start.4
  236.0 1.5 copy-start.11
  236.5 2.4 copy-start.13
  237.5 1.8 copy-start.33
  238.9 4.1 %copy-start.25 = (f32[3,256]{1,0:T(4,128)S(1)}, f32[3,256]{1,0:T(4,128)}, u32[]{:S(2)}) copy-start(f32[3,256]{1,0:T(4,128)} %param.28) | copy-start | bytes 9220
  239.7 4.8 %collective-permute-start = (bf16[2,256]{0,1:T(8,128)(2,1)S(1)}, bf16[2,256]{0,1:T(8,128)(2,1)S(1)}, u32[]{:S(2)}, u32[]{:S(2)}) collective-permute-start(bf16[2,256]{0,1:T(8,128)(2,1)S(1)} %slice.297), channel_id=1, source_target_pairs={{0,32},{32,64},{64,96},{96,128},{128,160},{160,192},{192,224},{224... | collective-permute-start | bytes 3080 | tf_op jit(solution)/shard_map/ppermute | solution.py:78
Sparse Core Ops, SparseCore 0:
  11.1 149.2 all-gather.2
Sparse Core Ops, SparseCore 1:
  190.8 81.6 all-gather.4
where the time goes:
time: 308 us; the launch traced here: 307 us
  waiting for transfers between devices  147 us (48%)
  blocking collectives  75.7 us (25%)
  local copies, waits for them, and re-layouts  26.1 us (8%)
  other arithmetic  16.3 us (5%)
  between operations  15.6 us (5%)
  matrix products  15.3 us (5%)
  starting transfers between devices  10.2 us (3%)
    all_gather x1, waiting for transfers between devices, local(): lax.all_gather(stacked, ('sp', 'fs'), axis=0, tiled=True)  113 us
    all_to_all x4, blocking collectives, from_everyone(): return lax.all_to_all(copies, axis, split_axis=0, concat_axis=0, tiled=True)  65.9 us
    all_to_all x1, waiting for transfers between devices, from_everyone(): return lax.all_to_all(copies, axis, split_axis=0, concat_axis=0, tiled=True)  33.2 us
    dot_general x2, matrix products, add_product(): return jnp.dot(left, piece, preferred_element_type=jnp.float32)  12.7 us
    all_gather x1, blocking collectives, whole_of(): array = lax.all_gather(array, axis, axis=dim, tiled=True)  9.85 us
    slice x3, local copies, waits for them, and re-layouts, sent_together(): done.append(lax.slice_in_dim(filled, at, at + a.shape[along], axis=along))  7.98 us
    all_to_all x1, starting transfers between devices, from_everyone(): return lax.all_to_all(copies, axis, split_axis=0, concat_axis=0, tiled=True)  6.94 us
  transfers between devices with their start and end apart: 4, of which 3 were waited for; matrix products, arithmetic and copies ran while one was open for 12% of the time, Pallas kernels for 0%

commit v1 on v0

v1 whole, which is shorter than its diff:
```python
import jax
import jax.numpy as jnp
from jax import lax
from jax.experimental import pallas as pl
from jax.experimental.pallas import tpu as pltpu
from jax.sharding import Mesh
from jax.sharding import PartitionSpec as P

DK = 64
DV = 128
BLOCK = 128
KERNEL = 3
TP = ("tp_0", "tp_1")
EPSILON = 1e-06
HIGHEST = lax.Precision.HIGHEST
MESH = pl.DeviceIdType.MESH
F32, BF16 = jnp.float32, jnp.bfloat16

VALUE, KEY, GATE, OUTGATE, EXIT, ENTRY, QUERY, WIDE = 0, 256, 384, 512, 768, 1024, 1280, 1408
COPIES = 208


class Wire:
    def __init__(self, sends, receives, anyone):
        self.sends, self.receives, self.anyone = sends, receives, anyone
        self.slots, self.started = {}, []

    def _copy(self, key, ref, device):
        slot = self.slots.setdefault(key, len(self.slots))
        assert slot < COPIES
        return pltpu.make_async_remote_copy(
            src_ref=ref,
            dst_ref=ref,
            send_sem=self.sends.at[slot],
            recv_sem=self.receives.at[slot],
            device_id=device,
            device_id_type=MESH,
        )

    def send(self, key, ref, device):
        copy = self._copy(key, ref, device)
        copy.start()
        self.started.append(copy)

    def wait(self, key, ref):
        self._copy(key, ref, self.anyone).wait_recv()

    def finish(self):
        for copy in self.started:
            copy.wait_send()


class Row:
    def __init__(self, wire, name, buffer, x, core, east, west, twin):
        self.wire, self.name, self.buffer = wire, name, buffer
        self.x, self.core, self.east, self.west, self.twin = x, core, east, west, twin

    def at(self, step, half=None, other=False):
        core = 1 - self.core if other else self.core
        slot = 2 * lax.rem(self.x + step + 4, 4) + core
        rows = self.buffer.shape[1] // 2
        if half is None:
            return self.buffer.at[slot]
        return self.buffer.at[slot, pl.ds(half * rows, rows), :]

    def start(self):
        self.wire.send((self.name, "e"), self.at(0), self.east)
        self.wire.send((self.name, "w"), self.at(0), self.west)
        self.wire.send((self.name, "t", 0), self.at(0), self.twin)

    def relay(self):
        self.wire.wait((self.name, "e"), self.at(-1))
        self.wire.send((self.name, "ee"), self.at(-1, 0), self.east)
        self.wire.send((self.name, "t", -1), self.at(-1), self.twin)
        self.wire.wait((self.name, "w"), self.at(1))
        self.wire.send((self.name, "ww"), self.at(1, 1), self.west)
        self.wire.send((self.name, "t", 1), self.at(1), self.twin)

    def hand_over(self):
        self.wire.wait((self.name, "ee"), self.at(2, 0))
        self.wire.wait((self.name, "ww"), self.at(2, 1))
        self.wire.send((self.name, "t", 2), self.at(2), self.twin)

    def complete(self):
        for step in (0, -1, 1, 2):
            self.wire.wait((self.name, "t", step), self.at(step, other=True))


class Wide:
    def __init__(self, wire, buffer, z, y, up, down, right, left):
        self.wire, self.buffer, self.z, self.y = wire, buffer, z, y
        self.up, self.down, self.right, self.left = up, down, right, left
        self.fresh, self.relayed = [], []

    def at(self, zs, ys, half=None):
        index = 4 * lax.rem(self.z + zs + 16, 16) + lax.rem(self.y + ys + 4, 4)
        if half is None:
            return self.buffer.at[pl.ds(pl.multiple_of(32 * index, 32), 32), :]
        return self.buffer.at[pl.ds(pl.multiple_of(32 * index + 16 * half, 16), 16), :]

    def round(self, r):
        wire = self.wire
        fresh = []
        if r == 0:
            fresh = [0]
        elif r < 8:
            wire.wait(("zu", r), self.at(-r, 0))
            wire.wait(("zd", r), self.at(r, 0))
            fresh = [-r, r]
        elif r == 8:
            wire.wait(("zu", r), self.at(8, 0, 0))
            wire.wait(("zd", r), self.at(8, 0, 1))
            fresh = [8]
        if r < 7:
            wire.send(("zu", r + 1), self.at(-r, 0), self.up)
            wire.send(("zd", r + 1), self.at(r, 0), self.down)
        elif r == 7:
            wire.send(("zu", r + 1), self.at(-r, 0, 0), self.up)
            wire.send(("zd", r + 1), self.at(r, 0, 1), self.down)
        for zs in fresh:
            wire.send(("yr", zs), self.at(zs, 0), self.right)
            wire.send(("yl", zs), self.at(zs, 0), self.left)
        for zs in self.fresh:
            wire.wait(("yr", zs), self.at(zs, -1))
            wire.send(("yrr", zs), self.at(zs, -1, 0), self.right)
            wire.wait(("yl", zs), self.at(zs, 1))
            wire.send(("yll", zs), self.at(zs, 1, 1), self.left)
        for zs in self.relayed:
            wire.wait(("yrr", zs), self.at(zs, 2, 0))
            wire.wait(("yll", zs), self.at(zs, 2, 1))
        self.fresh, self.relayed = fresh, self.fresh


class Narrow:
    def __init__(self, wire, name, buffer, rows, z, y, up, down, right, left):
        self.wire, self.name, self.buffer, self.rows, self.z, self.y = wire, name, buffer, rows, z, y
        self.up, self.down, self.right, self.left = up, down, right, left

    def item(self, ys, half=None):
        rows = self.rows
        index = 4 * self.z + lax.rem(self.y + ys + 4, 4)
        if half is None:
            return self.buffer.at[pl.ds(pl.multiple_of(rows * index, rows), rows), :]
        start = pl.multiple_of(rows * index + rows // 2 * half, rows // 2)
        return self.buffer.at[pl.ds(start, rows // 2), :]

    def block(self, zs, half=None):
        rows = 4 * self.rows
        index = lax.rem(self.z + zs + 16, 16)
        if half is None:
            return self.buffer.at[pl.ds(pl.multiple_of(rows * index, rows), rows), :]
        start = pl.multiple_of(rows * index + rows // 2 * half, rows // 2)
        return self.buffer.at[pl.ds(start, rows // 2), :]

    def round(self, r):
        wire, name = self.wire, self.name
        if r == 0:
            wire.send((name, "r"), self.item(0), self.right)
            wire.send((name, "l"), self.item(0), self.left)
            return
        if r == 1:
            wire.wait((name, "r"), self.item(-1))
            wire.send((name, "rr"), self.item(-1, 0), self.right)
            wire.wait((name, "l"), self.item(1))
            wire.send((name, "ll"), self.item(1, 1), self.left)
            return
        s = r - 2
        if s == 0:
            wire.wait((name, "rr"), self.item(2, 0))
            wire.wait((name, "ll"), self.item(2, 1))
        elif s < 8:
            wire.wait((name, "u", s), self.block(-s))
            wire.wait((name, "d", s), self.block(s))
        elif s == 8:
            wire.wait((name, "u", s), self.block(8, 0))
            wire.wait((name, "d", s), self.block(8, 1))
        if s < 7:
            wire.send((name, "u", s + 1), self.block(-s), self.up)
            wire.send((name, "d", s + 1), self.block(s), self.down)
        elif s == 7:
            wire.send((name, "u", s + 1), self.block(-s, 0), self.up)
            wire.send((name, "d", s + 1), self.block(s, 1), self.down)


class Column:
    def __init__(self, wire, buffer, z, up, down):
        self.wire, self.buffer, self.z, self.up, self.down = wire, buffer, z, up, down

    def at(self, zs, half=None):
        index = lax.rem(self.z + zs + 16, 16)
        if half is None:
            return self.buffer.at[index]
        return self.buffer.at[index, pl.ds(80 * half, 80 - 16 * half), :]

    def round(self, s):
        wire = self.wire
        if 0 < s < 8:
            wire.wait(("su", s), self.at(-s))
            wire.wait(("sd", s), self.at(s))
        elif s == 8:
            wire.wait(("su", s), self.at(8, 0))
            wire.wait(("sd", s), self.at(8, 1))
        if s < 7:
            wire.send(("su", s + 1), self.at(-s), self.up)
            wire.send(("sd", s + 1), self.at(s), self.down)
        elif s == 7:
            wire.send(("su", s + 1), self.at(-s, 0), self.up)
            wire.send(("sd", s + 1), self.at(s, 1), self.down)


def terms(value):
    first = value.astype(BF16).astype(F32)
    second = (value - first).astype(BF16).astype(F32)
    third = (value - first - second).astype(BF16).astype(F32)
    return first, second, third


def kernel(
    tokens, key_w, value_w, gate_w, query_w, outgate_w, exit_w, entry_w, signal_w, merge_w,
    gain, bias, shift, head_gain, taps,
    out,
    tok, wide, narrow, merge, normed, keys, values, gates, queries, outgates, exits,
    padded, rim, prefix, states, memory, conv, total,
    sends, receives, locals_,
):
    z, y = lax.axis_index("sp"), lax.axis_index("fs")
    x, core = lax.axis_index("tp_0"), lax.axis_index("tp_1")
    up, down = {"sp": lax.rem(z + 1, 16)}, {"sp": lax.rem(z + 15, 16)}
    right, left = {"fs": lax.rem(y + 1, 4)}, {"fs": lax.rem(y + 3, 4)}
    east, west = {"tp_0": lax.rem(x + 1, 4)}, {"tp_0": lax.rem(x + 3, 4)}
    twin = {"tp_1": 1 - core}
    own = 2 * x + core
    here = 4 * z + y

    barrier = pltpu.get_barrier_semaphore()
    for device in (up, down, right, left, east, west, twin):
        pl.semaphore_signal(barrier, inc=1, device_id=device, device_id_type=MESH)

    mine = pl.ds(pl.multiple_of(32 * here, 32), 32)
    loads = [
        (value_w, wide.at[mine, pl.ds(VALUE, 256)]),
        (key_w, wide.at[mine, pl.ds(KEY, 128)]),
        (gate_w, wide.at[mine, pl.ds(GATE, 128)]),
        (outgate_w, wide.at[mine, pl.ds(OUTGATE, 256)]),
        (exit_w, wide.at[mine, pl.ds(EXIT, 256)]),
        (entry_w, wide.at[mine, pl.ds(ENTRY, 256)]),
        (query_w, wide.at[mine, pl.ds(QUERY, 128)]),
        (signal_w, narrow.at[mine, :]),
        (merge_w, merge.at[pl.ds(pl.multiple_of(64 * here, 64), 64), :]),
        (tokens, tok.at[own]),
    ]
    loads = [pltpu.make_async_copy(src, dst, locals_.at[k]) for k, (src, dst) in enumerate(loads)]
    for load in loads:
        load.start()
    pl.semaphore_wait(barrier, 7)
    for load in loads:
        load.wait()

    wire = Wire(sends, receives, up)
    row_tok = Row(wire, "tok", tok, x, core, east, west, twin)
    row_conv = Row(wire, "conv", conv, x, core, east, west, twin)
    row_memory = Row(wire, "memory", memory, x, core, east, west, twin)
    wide_ring = Wide(wire, wide, z, y, up, down, right, left)
    signal_ring = Narrow(wire, "signal", narrow, 32, z, y, up, down, right, left)
    merge_ring = Narrow(wire, "merge", merge, 64, z, y, up, down, right, left)
    column = Column(wire, states, z, up, down)

    for r in range(11):
        wide_ring.round(r)
        signal_ring.round(r)
        merge_ring.round(r)
        if r == 0:
            row_tok.start()
        if r == 1:
            row_tok.relay()
        if r == 2:
            row_tok.hand_over()
        if r == 3:
            row_tok.complete()

            def norm_rows(i, _):
                rows = pl.ds(pl.multiple_of(16 * i, 16), 16)
                parts = [tok[t, rows, :].astype(F32) for t in range(8)]
                squares = parts[0] * parts[0]
                for part in parts[1:]:
                    squares = squares + part * part
                mean = jnp.sum(squares, axis=-1, keepdims=True) * (1.0 / 2048)
                factor = lax.rsqrt(mean + EPSILON)
                for t, part in enumerate(parts):
                    columns = slice(256 * t, 256 * t + 256)
                    normed[rows, columns] = (part * factor * gain[:, columns]).astype(BF16)
                return 0

            lax.fori_loop(0, 32, norm_rows, 0)

    def product(weights, start, width):
        return jnp.dot(
            normed[...], weights[:, start : start + width], preferred_element_type=F32
        )

    values[...] = product(wide, VALUE, 256).astype(BF16)
    both = product(wide, KEY, 256)
    keys[...] = both[:, :128].astype(BF16)
    gates[...] = both[:, 128:]

    lane = lax.broadcasted_iota(jnp.int32, (8, 128), 1)
    line = lax.broadcasted_iota(jnp.int32, (8, 128), 0)
    turned = [gates[128 * c : 128 * c + 128, :].T for c in range(4)]
    inputs = jnp.concatenate([part[0:2] for part in turned], axis=0)
    forgets = jnp.concatenate([part[2:4] for part in turned], axis=0)
    shifts = jnp.concatenate([shift[:, 128 * c : 128 * c + 128] for c in range(4)], axis=0)
    forgets = forgets + jnp.where(lax.rem(line, 2) == 0, bias[0], bias[1])
    cumulative = jnp.minimum(forgets, 0.0) - jnp.log1p(jnp.exp(-jnp.abs(forgets))) + shifts
    for k in (1, 2, 4, 8, 16, 32, 64):
        cumulative = cumulative + jnp.where(lane >= k, pltpu.roll(cumulative, k, 1), 0.0)
    last = cumulative[:, 127:128]
    weight_logs = last - cumulative + inputs
    peak = jnp.max(weight_logs, axis=1, keepdims=True)
    coefficients = jnp.exp(weight_logs - peak)
    upright = jnp.concatenate([cumulative, coefficients, jnp.zeros((112, 128), F32)], axis=0).T

    lanes = lax.broadcasted_iota(jnp.int32, (128, 128), 1)
    lines = lax.broadcasted_iota(jnp.int32, (128, 128), 0)

    def by_line(pair):
        return jnp.where(lines < DK, pair[0], pair[1])

    def joined(earlier, later):
        ceilings = [jnp.maximum(b + m, n) for m, n, b in zip(earlier[1], later[1], later[2])]
        kept = [jnp.exp(b + m - c) for m, b, c in zip(earlier[1], later[2], ceilings)]
        added = [jnp.exp(n - c) for n, c in zip(later[1], ceilings)]
        state = by_line(kept) * earlier[0] + by_line(added) * later[0]
        return state, ceilings, [a + b for a, b in zip(earlier[2], later[2])]

    running, marks = None, []
    for c in range(4):
        block = slice(128 * c, 128 * c + 128)
        factors = [upright[:, 8 + 2 * c + h : 9 + 2 * c + h] for h in range(2)]
        weighted_keys = (
            keys[block, :].astype(F32) * DK**-0.5 * jnp.where(lanes < DK, factors[0], factors[1])
        )
        outer = lax.dot_general(
            weighted_keys,
            values[block, :].astype(F32),
            (((0,), (0,)), ((), ())),
            precision=HIGHEST,
            preferred_element_type=F32,
        )
        state = jnp.where(lines < DK, outer[:, :128], outer[:, 128:])
        piece = (
            state,
            [peak[2 * c + h : 2 * c + h + 1, :] for h in range(2)],
            [last[2 * c + h : 2 * c + h + 1, :] for h in range(2)],
        )
        if running is None:
            running = piece
        else:
            prefix[c - 1] = running[0]
            marks.append(running[1:])
            running = joined(running, piece)

    states[z, 0:128, :] = running[0].astype(BF16)
    parts = [part for value in (*running[1], *running[2]) for part in terms(value)]
    lines16 = lax.broadcasted_iota(jnp.int32, (16, 128), 0)
    packed = jnp.zeros((16, 128), F32)
    for k, part in enumerate(parts):
        packed = jnp.where(lines16 == k, part, packed)
    states[z, 128:144, :] = packed.astype(BF16)
    column.round(0)

    entries = product(wide, ENTRY, 256).astype(BF16).astype(F32)
    signals = product(narrow, 0, 256).astype(BF16).astype(F32)
    mixed_in = (entries * signals).astype(BF16)
    padded[16:528, :] = mixed_in.astype(F32)
    rim[pl.ds(0, 1)] = mixed_in[496:512, :][None]
    rim_copy = pltpu.make_async_remote_copy(
        src_ref=rim.at[0],
        dst_ref=rim.at[1],
        send_sem=sends.at[COPIES],
        recv_sem=receives.at[COPIES],
        device_id=up,
        device_id_type=MESH,
    )
    rim_copy.start()
    column.round(1)
    exits[...] = product(wide, EXIT, 256).astype(BF16)
    column.round(2)
    rim_copy.wait()
    padded[0:16, :] = jnp.where(z > 0, rim[1].astype(F32), 0.0)
    response = taps[0:1, :] * padded[14:526, :]
    for tap in range(1, KERNEL):
        response = response + taps[tap : tap + 1, :] * padded[14 + tap : 526 + tap, :]
    conv[own] = (exits[...].astype(F32) * response).astype(BF16)
    row_conv.start()
    column.round(3)
    outgates[...] = product(wide, OUTGATE, 256).astype(BF16)
    column.round(4)
    queries[...] = product(wide, QUERY, 128).astype(BF16)
    column.round(5)
    column.round(6)
    row_conv.relay()
    column.round(7)
    column.round(8)

    carried = (jnp.zeros((128, 128), F32), [jnp.zeros((1, 1), F32)] * 2)
    for u in range(16):
        packed = states[u, 128:144, :].astype(F32)
        sums = [
            packed[3 * k : 3 * k + 1, 0:1]
            + packed[3 * k + 1 : 3 * k + 2, 0:1]
            + packed[3 * k + 2 : 3 * k + 3, 0:1]
            for k in range(4)
        ]
        passed = u < z
        ceilings, kept, added = [], [], []
        for m, n, b in zip(carried[1], sums[0:2], sums[2:4]):
            ceiling = jnp.maximum(b + m, n)
            kept.append(jnp.where(passed, jnp.exp(b + m - ceiling), 1.0))
            added.append(jnp.where(passed, jnp.exp(n - ceiling), 0.0))
            ceilings.append(jnp.where(passed, ceiling, m))
        state = by_line(kept) * carried[0] + by_line(added) * states[u, 0:128, :].astype(F32)
        carried = (state, ceilings)

    for c in range(4):
        block = slice(128 * c, 128 * c + 128)
        before = carried
        if c > 0:
            before = joined((*carried, [0.0, 0.0]), (prefix[c - 1], *marks[c - 1]))
        query, key = queries[block, :], keys[block, :]
        for h in range(2):
            k = 2 * c + h
            head = slice(128 * h, 128 * h + 128)
            column_b = upright[:, k : k + 1]
            decay = column_b - cumulative[k : k + 1, :] + inputs[k : k + 1, :]
            decay = jnp.where(lanes <= lines, decay, -jnp.inf)
            inter = column_b + before[1][h]
            ceiling = jnp.maximum(inter, jnp.max(decay, axis=-1, keepdims=True))
            chosen = (lanes < DK) if h == 0 else (lanes >= DK)
            masked = jnp.where(chosen, query.astype(F32), 0.0)
            scores = lax.dot_general(
                masked.astype(BF16), key, (((1,), (1,)), ((), ())), preferred_element_type=F32
            )
            weighted = (scores * DK**-0.5 * jnp.exp(decay - ceiling)).astype(BF16)
            numerator = jnp.dot(weighted, values[block, head], preferred_element_type=F32)
            numerator = numerator + jnp.exp(inter - ceiling) * jnp.dot(
                masked, before[0], precision=HIGHEST, preferred_element_type=F32
            )
            mean = jnp.mean(numerator * numerator, axis=-1, keepdims=True)
            hidden = numerator * lax.rsqrt(mean + EPSILON) * head_gain[:, head]
            gate = outgates[block, head].astype(F32)
            memory[own, block, head] = (hidden / (1.0 + jnp.exp(-gate))).astype(BF16)
    row_memory.start()

    def merged(buffer, offset):
        result = None
        for t in range(8):
            rows = slice(offset + 256 * t, offset + 256 * t + 256)
            term = jnp.dot(buffer[t], merge[rows, :], preferred_element_type=F32)
            result = term if result is None else result + term
        return result

    row_conv.hand_over()
    row_conv.complete()
    total[...] = merged(conv, 2048)
    row_memory.relay()
    row_memory.hand_over()
    row_memory.complete()
    out[...] = (total[...] + merged(memory, 0)).astype(BF16)
    wire.finish()


def local(
    tokens,
    norm_gain,
    query_weight,
    key_weight,
    value_weight,
    outgate_weight,
    gate_weight,
    forget_bias,
    forget_shift,
    head_norm_gain,
    exit_weight,
    entry_weight,
    signal_weight,
    conv_kernel,
    merge_weight,
):
    gate_rows = jnp.pad(gate_weight.reshape(32, 4), ((0, 0), (0, 124)))
    hbm = pl.BlockSpec(memory_space=pl.ANY)
    vmem = pl.BlockSpec(memory_space=pltpu.VMEM)
    smem = pl.BlockSpec(memory_space=pltpu.SMEM)
    mixed = pl.pallas_call(
        kernel,
        out_shape=jax.ShapeDtypeStruct((512, 256), BF16),
        in_specs=[hbm] * 10 + [vmem, smem, vmem, vmem, vmem],
        out_specs=vmem,
        scratch_shapes=[
            pltpu.VMEM((8, 512, 256), BF16),
            pltpu.VMEM((2048, WIDE), BF16),
            pltpu.VMEM((2048, 256), BF16),
            pltpu.VMEM((4096, 256), BF16),
            pltpu.VMEM((512, 2048), BF16),
            pltpu.VMEM((512, 128), BF16),
            pltpu.VMEM((512, 256), BF16),
            pltpu.VMEM((512, 128), F32),
            pltpu.VMEM((512, 128), BF16),
            pltpu.VMEM((512, 256), BF16),
            pltpu.VMEM((512, 256), BF16),
            pltpu.VMEM((528, 256), F32),
            pltpu.VMEM((2, 16, 256), BF16),
            pltpu.VMEM((3, 128, 128), F32),
            pltpu.VMEM((16, 144, 128), BF16),
            pltpu.VMEM((8, 512, 256), BF16),
            pltpu.VMEM((8, 512, 256), BF16),
            pltpu.VMEM((512, 256), F32),
            pltpu.SemaphoreType.DMA((COPIES + 1,)),
            pltpu.SemaphoreType.DMA((COPIES + 1,)),
            pltpu.SemaphoreType.DMA((10,)),
        ],
        compiler_params=pltpu.CompilerParams(
            collective_id=0, has_side_effects=True, vmem_limit_bytes=56 * 1024 * 1024
        ),
        name="layer",
    )(
        tokens[0], key_weight, value_weight, gate_rows, query_weight, outgate_weight,
        exit_weight, entry_weight, signal_weight, merge_weight,
        norm_gain[None], forget_bias, forget_shift[0], head_norm_gain[None], conv_kernel,
    )
    return mixed[None]


def solution(mesh):
    assert (mesh.shape["sp"], mesh.shape["fs"], mesh.shape["tp"]) == (16, 4, 8)
    torus = Mesh(mesh.devices.reshape(16, 4, 4, 2), ("sp", "fs", "tp_0", "tp_1"))
    in_specs = (
        P("fs", "sp", TP),
        P(),
        P(("sp", "fs"), TP),
        P(("sp", "fs"), TP),
        P(("sp", "fs"), TP),
        P(("sp", "fs"), TP),
        P(("sp", "fs"), None, TP),
        P(TP),
        P("fs", TP, "sp"),
        P(TP),
        P(("sp", "fs"), TP),
        P(("sp", "fs"), TP),
        P(("sp", "fs"), TP),
        P(None, TP),
        P(("sp", "fs"), TP),
    )
    out_specs = P("fs", "sp", TP)
    return jax.shard_map(local, mesh=torus, in_specs=in_specs, out_specs=out_specs, check_vma=False)
```

time: 308 us -> 129 us (0.42)
  waiting for transfers between devices: 147 us -> 0 us
  Pallas kernels: 0 us -> 125 us
  blocking collectives: 75.7 us -> 0 us
  local copies, waits for them, and re-layouts: 26.1 us -> 3.06 us
  other arithmetic: 16.3 us -> 0 us
  between operations: 15.6 us -> 0.01 us
  matrix products: 15.3 us -> 0 us
  starting transfers between devices: 10.2 us -> 0 us
    pallas_call x0 -> x1, Pallas kernels: none -> 125 us  [local(): pl.pallas_call(kernel, out_shape=jax.ShapeDtypeStruct((512, 256), BF16),...]
    all_gather x2 -> x0, waiting for transfers between devices: 113 us -> none  [the longest x1 113 us: local(): lax.all_gather(stacked, ('sp', 'fs'), axis=0, tiled=True)]
    all_to_all x4 -> x0, blocking collectives: 65.9 us -> none  [from_everyone(): return lax.all_to_all(copies, axis, split_axis=0, concat_axis=0, tiled=True)]
    all_to_all x1 -> x0, waiting for transfers between devices: 33.2 us -> none  [from_everyone(): return lax.all_to_all(copies, axis, split_axis=0, concat_axis=0, tiled=True)]
    dot_general x5 -> x0, matrix products: 15.3 us -> none  [the longest x2 12.7 us: add_product(): return jnp.dot(left, piece, preferred_element_type=jnp.float32)]
    all_gather x1 -> x0, blocking collectives: 9.85 us -> none  [whole_of(): array = lax.all_gather(array, axis, axis=dim, tiled=True)]
    slice x22 -> x0, local copies, waits for them, and re-layouts: 8.48 us -> none  [the longest x3 7.98 us: sent_together(): done.append(lax.slice_in_dim(filled, at, at + a.shape[along], axis=along))]
    all_to_all x1 -> x0, starting transfers between devices: 6.94 us -> none  [from_everyone(): return lax.all_to_all(copies, axis, split_axis=0, concat_axis=0, tiled=True)]
  transfers between devices with their start and end apart: 4 -> 0, of which waited for: 3 -> 0; matrix products, arithmetic and copies ran while one was open for 12% -> 0% of each run, Pallas kernels for 0% -> 0%
where the time goes in v1:
time: 129 us; the launch traced here: 128 us
  Pallas kernels  125 us (97%)
  local copies, waits for them, and re-layouts  3.06 us (2%)
    pallas_call x1, Pallas kernels, local(): pl.pallas_call(kernel, out_shape=jax.ShapeDtypeStruct((512, 256), BF16),...  125 us

profile of v1, /device:TPU:1, one launch (start us, length us, event | category | flops | bytes accessed | tf_op | source)
XLA Modules:
  0.0 128.4 jit_solution(14020543369801708743)
XLA Ops:
  0.0 0.0 copy-start
  0.0 0.7 copy-done
  0.7 0.1 copy.16
  0.8 0.6 pad.4.gate_w
  1.4 125.4 %layer.1 = bf16[512,256]{1,0:T(8,128)(2,1)} custom-call(bf16[512,256]{1,0:T(8,128)(2,1)} %bitcast.7, bf16[32,128]{1,0:T(8,128)(2,1)} %key_w.1, bf16[32,256]{1,0:T(8,128)(2,1)} %value_w.1, bf16[32,128]{1,0:T(8,128)(2,1)} %pad.4.gate_w, bf16[32,128]{1,0:T(8,128)(2,1)} %query_w.1, bf16[32,256]{1,0:T(8,128)(2,1)} %outgate_w.1, bf16[32,256]{1,0:T(8,128)(2,1)} %exit_w.1, ...), custom_call_target="tpu_custom_call" | custom-call | tf_op jit(solution)/shard_map/layer/pallas_call | solution.py:493
  126.8 1.7 %copy.18 = bf16[1,512,256]{2,1,0:T(8,128)(2,1)} copy(bf16[1,512,256]{2,1,0:T(8,128)(2,1)} %bitcast.6) | data formatting | bytes 524288
Async XLA Ops:
  0.0 0.7 copy-start
